TPU v7x, 32 devices: a whole 2x2x4 slice. The times are simulated.
32 devices in a mesh: rep: 4 (over z), fs: 4 (over y, x), tp: 2 (over core).
Axes of the slice: x: 2, y: 2, z: 4, core: 2. Of those that a mesh axis runs over, the one named last changes fastest.
Arguments:
- pre_gate: bfloat16 [3072, 7936], P('rep', ('fs', 'tp')), may hold values from -6 to 6
- pre_up: bfloat16 [3072, 7936], P('rep', ('fs', 'tp')), may hold values from -6 to 6
- cotangent: bfloat16 [3072, 4096], P('rep', ('fs', 'tp')), may hold values from -6 to 6
- down_weight: bfloat16 [7936, 4096], P(('fs', 'tp')), may hold values from -0.0625 to 0.0625
Outputs:
- grad_gate: bfloat16 [3072, 7936], P('rep', ('fs', 'tp'))
- grad_up: bfloat16 [3072, 7936], P('rep', ('fs', 'tp'))
- grad_down: float32 [7936, 4096], P(('fs', 'tp'), 'rep')
- row_squares: float32 [7936], P(('fs', 'tp'))
All inputs are finite; a program needn't handle non-finite values.
Results may differ from a plain program's by a relative error of at most 0.0034.
Values may be sent and summed in bfloat16 or wider, within the bound.
No kernel may reach another device: no remote copies, remote signals or barrier semaphores. Data moves between devices by JAX's collectives and lax.ppermute only.
A program may use at most 128 MiB of HBM per device.

v0:
```python
import jax
import jax.numpy as jnp
from jax import lax
from jax.sharding import PartitionSpec as P


def local(pre_gate, pre_up, cotangent, down_weight):
    gate_wide = pre_gate.astype(jnp.float32)
    up_wide = pre_up.astype(jnp.float32)
    sigmoid_gate = jax.nn.sigmoid(gate_wide)
    act = gate_wide * sigmoid_gate
    hidden = (act * up_wide).astype(jnp.bfloat16)
    piece = lax.all_gather(cotangent, ("fs", "tp"), axis=1, tiled=True)
    partial_grad = lax.dot_general(
        piece, down_weight, (((1,), (1,)), ((), ())), preferred_element_type=jnp.float32
    )
    block = lax.dot_general(
        piece, hidden, (((0,), (0,)), ((), ())), preferred_element_type=jnp.float32
    )
    grad_up = (partial_grad * act).astype(jnp.bfloat16)
    slope = sigmoid_gate * (1.0 + gate_wide * (1.0 - sigmoid_gate))
    grad_gate = (partial_grad * up_wide * slope).astype(jnp.bfloat16)
    shard_rows = lax.psum_scatter(block, "rep", scatter_dimension=0, tiled=True)
    grad_down = shard_rows.T
    partial_squares = jnp.sum(grad_down * grad_down, axis=1)
    row_squares = lax.psum(partial_squares, "rep")
    return (grad_gate, grad_up, grad_down, row_squares)


def solution(mesh):
    placed = (
        P("rep", ("fs", "tp")),
        P("rep", ("fs", "tp")),
        P("rep", ("fs", "tp")),
        P(("fs", "tp"), None),
    )
    return jax.shard_map(
        local,
        mesh=mesh,
        in_specs=placed,
        out_specs=(
            P("rep", ("fs", "tp")),
            P("rep", ("fs", "tp")),
            P(("fs", "tp"), "rep"),
            P(("fs", "tp")),
        ),
        check_vma=False,
    )
```

profile of v0, /device:TPU:0, one launch (start us, length us, event | category | flops | bytes accessed | tf_op | source)
XLA Modules:
  0.0 365.5 jit_solution(954260564306209259)
XLA Ops:
  7.2 0.0 all-gather.2.cloned.1.call-start
  7.2 0.7 all-gather.2.cloned.1.call-update
  7.9 0.0 reduce-scatter.2.cloned.1.call-start
  7.9 51.2 %all-gather.2.cloned.1.call-done = bf16[768,4096]{1,0:T(8,128)(2,1)} async-done(((bf16[768,512]{1,0:T(8,128)(2,1)}), bf16[768,4096]{1,0:T(8,128)(2,1)}) %all-gather.2.cloned.1.call-update) | async-done | bytes 6291472 | tf_op jit(solution)/shard_map/all_gather | solution.py:13
  59.2 13.2 %convolution_bitcast_fusion = f32[4096,992]{0,1:T(8,128)} fusion(bf16[768,4096]{1,0:T(8,128)(2,1)} %all-gather.2.cloned.1.call-done, bf16[768,992]{0,1:T(8,128)(2,1)} %param.5, bf16[768,992]{0,1:T(8,128)(2,1)} %param.4), kind=kOutput, calls=%fused_computation | convolution fusion | flops 6247219200 | bytes 25591808 | tf_op jit(solution)/shard_map/dot_general | solution.py:17
  72.3 0.0 copy-start
  72.3 0.0 copy-start.1
  72.3 0.0 reduce-scatter.2.cloned.1.call-update
  72.4 1.4 copy-done
  73.7 0.5 copy-done.1
  74.2 12.8 %multiply_convert_fusion = (bf16[768,992]{0,1:T(8,128)(2,1)}, bf16[768,992]{0,1:T(8,128)(2,1)}) fusion(bf16[768,992]{0,1:T(8,128)(2,1)S(1)} %copy-done, bf16[768,992]{0,1:T(8,128)(2,1)S(1)} %copy-done.1, bf16[768,4096]{1,0:T(8,128)(2,1)} %all-gather.2.cloned.1.call-done, bf16[992,4096]{1,0:T(8,128)(2,1)} %param.7), kind=kOutput, calls=%fused_computation.15 | convolution fusion | flops 6252552192 | bytes 20512768 | tf_op jit(solution)/shard_map/dot_general | solution.py:14
  87.0 257.7 %reduce-scatter.2.cloned.1.call-done = f32[1024,992]{0,1:T(8,128)} async-done(((f32[4096,992]{0,1:T(8,128)}), f32[1024,992]{0,1:T(8,128)}) %reduce-scatter.2.cloned.1.call-update) | async-done | bytes 4063248 | tf_op jit(solution)/shard_map/reduce_scatter | solution.py:23
  344.6 2.5 multiply_reduce_fusion
  347.1 11.6 %psum.7 = f32[992]{0:T(1024)} all-reduce(f32[992]{0:T(1024)S(1)} %multiply_reduce_fusion), channel_id=1, replica_groups=mesh['rep'=4,'fs'=4,'tp'=2] {'rep'}, use_global_device_ids=true, to_apply=%region_2.0 | all-reduce | flops 992 | bytes 7936 | tf_op jit(solution)/shard_map/psum | solution.py:26
Async XLA Ops:
  7.2 52.0 %all-gather.2.cloned.1.call-start = ((), (), s32[]{:S(2)}) async-start(), calls=%async_computation.1 | async-start | bytes 7077888 | tf_op jit(solution)/shard_map/all_gather | solution.py:13
  7.9 336.7 %reduce-scatter.2.cloned.1.call-start = ((), (), s32[]{:S(2)}) async-start(), calls=%async_computation.2 | async-start | bytes 20316160 | tf_op jit(solution)/shard_map/reduce_scatter | solution.py:23
  72.3 1.4 copy-start
  72.3 1.8 copy-start.1
Sparse Core Ops, SparseCore 0:
  9.8 49.2 all-gather.1
  72.5 272.0 reduce-scatter.1
where the time goes:
time: 366 us
  waiting for transfers between devices  310 us (85%)
  matrix products  25.9 us (7%)
  between operations  14 us (4%)
  blocking collectives  11.6 us (3%)
    reduce_scatter x1, waiting for transfers between devices, local(): shard_rows = lax.psum_scatter(block, 'rep', scatter_dimension=0, tiled=True)  258 us
    all_gather x1, waiting for transfers between devices, local(): piece = lax.all_gather(cotangent, ('fs', 'tp'), axis=1, tiled=True)  51.2 us
    dot_general x1, matrix products, local(): lax.dot_general(piece, hidden, (((0,), (0,)), ((), ())), preferred_elemen...  13.2 us
    dot_general x1, matrix products, local(): lax.dot_general(piece, down_weight, (((1,), (1,)), ((), ())), preferred_e...  12.8 us
    psum x1, blocking collectives, local(): row_squares = lax.psum(partial_squares, 'rep')  11.6 us
  transfers between devices with their start and end apart: 2, of which 2 were waited for; matrix products, arithmetic and copies ran while one was open for 3% of the time, Pallas kernels for 0%

commit v1 on v0

v1 whole, which is shorter than its diff:
```python
import jax
import jax.numpy as jnp
from jax import lax
from jax.experimental import pallas as pl
from jax.experimental.pallas import tpu as pltpu
from jax.sharding import PartitionSpec as P


F32 = jnp.float32
BF16 = jnp.bfloat16


def dot(a, b, ca, cb):
    return lax.dot_general(
        a, b, (((ca,), (cb,)), ((), ())), preferred_element_type=F32
    )


def elementwise(pre_gate, pre_up):
    gate = pre_gate.astype(F32)
    up = pre_up.astype(F32)
    sig = jax.nn.sigmoid(gate)
    act = gate * sig
    slope = sig * (1.0 + gate * (1.0 - sig))
    return act, up, slope


def general(pre_gate, pre_up, cotangent, down_weight):
    act, up, slope = elementwise(pre_gate, pre_up)
    hidden = (act * up).astype(BF16)
    piece = lax.all_gather(cotangent, ("fs", "tp"), axis=1, tiled=True)
    grad = dot(piece, down_weight, 1, 1)
    block = dot(piece, hidden, 0, 0)
    grad_up = (grad * act).astype(BF16)
    grad_gate = (grad * up * slope).astype(BF16)
    grad_down = lax.psum_scatter(block, "rep", scatter_dimension=0, tiled=True).T
    squares = lax.psum(jnp.sum(grad_down * grad_down, axis=1), "rep")
    return grad_gate, grad_up, grad_down, squares


def products(hiddens, own, partner, far, flags):
    width, rows = hiddens[0].shape
    block = own[0].shape[1]
    half = rows // 2

    def kernel(flags_ref, *refs):
        h_own, h_partner, h_far = refs[:3]
        own_refs, partner_refs, far_refs = refs[3:7], refs[7:15], refs[15:23]
        mate_ref, z_ref = refs[23:]
        near = pl.multiple_of(flags_ref[2], half)
        other = pl.multiple_of(half - flags_ref[2], half)

        def mul(a, b):
            return jnp.dot(a, b, preferred_element_type=F32)

        for core in range(2):
            column = pl.multiple_of((flags_ref[1] ^ core) * block, block)
            for at_x in range(2):
                total = mul(h_own[...], own_refs[2 * core + at_x][...])
                for h, group in ((h_partner, partner_refs), (h_far, far_refs)):
                    a, b = group[4 * core + at_x], group[4 * core + 2 + at_x]
                    total += mul(h[:, pl.ds(near, half)], a[...])
                    total += mul(h[:, pl.ds(other, half)], b[...])
                is_z = flags_ref[0] == 1 - at_x

                @pl.when(is_z)
                def _(total=total, column=column):
                    z_ref[:, pl.ds(column, block)] = total

                @pl.when(jnp.logical_not(is_z))
                def _(total=total, column=column):
                    mate_ref[:, pl.ds(column, block)] = total.astype(BF16)

    vmem = pl.BlockSpec(memory_space=pltpu.VMEM)
    flops = 2 * 3 * rows * width * 4 * block
    return pl.pallas_call(
        kernel,
        in_specs=[pl.BlockSpec(memory_space=pltpu.SMEM)] + [vmem] * 23,
        out_specs=[vmem, vmem],
        out_shape=[
            jax.ShapeDtypeStruct((width, 2 * block), BF16),
            jax.ShapeDtypeStruct((width, 2 * block), F32),
        ],
        cost_estimate=pl.CostEstimate(
            flops=flops, bytes_accessed=rows * block * 24, transcendentals=0
        ),
        name="products",
    )(flags, *hiddens, *own, *partner, *far)


def line(pre_gate, pre_up, shard, down_weight):
    z = lax.axis_index("rep")
    fs = lax.axis_index("fs")
    t = lax.axis_index("tp")
    y, x = fs >> 1, fs & 1
    rows = shard.shape[0]
    ff = pre_gate.shape[1]
    r2 = rows // 2
    own_half = z >> 1
    holds = y == own_half
    x_is_z = x == (z & 1)
    tie = lax.optimization_barrier

    def square(v, flip, who=lambda a, b: True):
        pairs = [
            (4 * a + b, 4 * a + (b ^ flip))
            for a in range(4)
            for b in range(4)
            if who(a, b)
        ]
        return lax.ppermute(v, ("rep", "fs"), pairs)

    def holder(a, b):
        return b >> 1 == a >> 1

    def other(a, b):
        return not holder(a, b)

    def to_t(v):
        return lax.ppermute(v, "tp", [(0, 1), (1, 0)])

    def to_partner(v):
        return lax.ppermute(v, "rep", [(1, 2), (2, 1)])

    def to_far(v):
        return lax.ppermute(v, "rep", [(0, 2), (3, 1)])

    def to_mate(v):
        return lax.ppermute(v, "rep", [(i, i ^ 1) for i in range(4)])

    def pair(first, a, b, axis):
        return jnp.concatenate(
            [jnp.where(first, a, b), jnp.where(first, b, a)], axis=axis
        )

    spans, start = [], 0
    for size in SPANS:
        stop = min(start + size, ff)
        if stop > start:
            spans.append((start, stop))
        start = stop

    top, bottom = shard[:r2], shard[r2:]
    yn_a = square(tie(top), 2, other)
    ys = square(shard, 2, holder)
    xn = square(shard, 1, holder)
    yo = square(shard, 2, other)
    cross = tie(jnp.where(holds, yn_a, bottom))

    parts = []
    for a, b in spans:
        gate, up = pre_gate[:, a:b].astype(F32), pre_up[:, a:b].astype(F32)
        parts.append(tie((gate * jax.nn.sigmoid(gate) * up).astype(BF16).T))
    h_partner = [to_partner(part) for part in parts]
    h_far = [to_far(part) for part in parts]
    q_partner = to_partner(cross)
    q_far = to_far(cross)

    yx = square(xn, 2, holder)
    ys, xn, yx, s1 = tie((ys, xn, yx, shard))
    own_x = jnp.where(holds, s1, ys)
    own_xn = jnp.where(holds, xn, yx)
    own_x, own_xn = tie((own_x, own_xn))
    own = (own_x, own_xn, to_t(own_x), to_t(own_xn))

    def spread(q, last):
        qx, qy = square(q, 1), square(q, 2)
        qd = square(qx if last == 2 else qy, last)
        four = (q, qx, qy, qd)
        return (*four, *[to_t(v) for v in four])

    partner, far = spread(q_partner, 1), spread(q_far, 2)
    flags = jnp.stack([x_is_z.astype(jnp.int32), t, jnp.where(holds, r2, 0)])

    yo, s2 = tie((yo, shard))
    oth_x = tie(jnp.where(holds, yo, s2))
    oth_xn = square(oth_x, 1)
    own_t, oth_t = own[2:], (to_t(oth_x), to_t(oth_xn))

    def columns(blocks, blocks_t):
        here = pair(t == 0, blocks[0], blocks_t[0], 1)
        there = pair(t == 0, blocks[1], blocks_t[1], 1)
        return pair(x == 0, here, there, 1)

    full = pair(
        own_half == 0, columns(own[:2], own_t), columns((oth_x, oth_xn), oth_t), 1
    )
    act, up, slope = elementwise(*tie((pre_gate, pre_up, full))[:2])
    grad = dot(full, down_weight, 1, 1)
    grad_up = (grad * act).astype(BF16)
    grad_gate = (grad * up * slope).astype(BF16)

    zs, backs = [], []
    for k in range(len(parts)):
        hiddens = (parts[k], h_partner[k], h_far[k])
        if k == len(parts) - 1:
            part, grad_up, grad_gate = tie((parts[k], grad_up, grad_gate))
            hiddens = (part, *hiddens[1:])
        mate_sum, own_sum = products(hiddens, own, partner, far, flags)
        backs.append(to_mate(mate_sum))
        zs.append(own_sum)
    downs, squares = [], []
    for own_sum, back in zip(zs, backs):
        down = own_sum + back.astype(F32)
        downs.append(down)
        squares.append(jnp.sum(down * down, axis=1))
    partial = jnp.concatenate(squares, axis=0)
    total = partial
    for shift in (1, 2, 3):
        total = total + lax.ppermute(
            partial, "rep", [(i, (i + shift) % 4) for i in range(4)]
        )
    return grad_gate, grad_up, jnp.concatenate(downs, axis=0), total


SPANS = (384, 384, 384)


def solution(mesh):
    sizes = dict(mesh.shape)
    placed = P("rep", ("fs", "tp"))

    def shard_mapped(body):
        return jax.shard_map(
            body,
            mesh=mesh,
            in_specs=(placed, placed, placed, P(("fs", "tp"), None)),
            out_specs=(placed, placed, P(("fs", "tp"), "rep"), P(("fs", "tp"))),
            check_vma=False,
        )

    if (sizes["rep"], sizes["fs"], sizes["tp"]) != (4, 4, 2):
        return shard_mapped(general)

    return shard_mapped(line)
```

time: 366 us -> 206 us (0.56)
  waiting for transfers between devices: 310 us -> 69.1 us
  starting transfers between devices: 0.08 us -> 77.5 us
  Pallas kernels: 0 us -> 30.2 us
  matrix products: 25.9 us -> 8.71 us
  between operations: 14 us -> 1.16 us
  blocking collectives: 11.6 us -> 0 us
  other arithmetic: 2.48 us -> 13.5 us
  local copies, waits for them, and re-layouts: 1.82 us -> 5.57 us
    reduce_scatter x1 -> x0, waiting for transfers between devices: 258 us -> none  [local(): shard_rows = lax.psum_scatter(block, 'rep', scatter_dimension=0, tiled=True)]
    ppermute x0 -> x38, starting transfers between devices: none -> 77.5 us  [the longest x4 31 us: to_far(): return lax.ppermute(v, 'rep', [(0, 2), (3, 1)])]
    ppermute x0 -> x38, waiting for transfers between devices: none -> 69.1 us  [the longest x12 35.9 us: square(): return lax.ppermute(v, ('rep', 'fs'), pairs)]
    all_gather x1 -> x0, waiting for transfers between devices: 51.2 us -> none  [local(): piece = lax.all_gather(cotangent, ('fs', 'tp'), axis=1, tiled=True)]
    pallas_call x0 -> x3, Pallas kernels: none -> 30.2 us  [products(): pl.pallas_call(kernel, in_specs=[pl.BlockSpec(memory_space=pltpu.SMEM)] +...]
    dot_general x2 -> x1, matrix products: 25.9 us -> 8.71 us  [dot(): lax.dot_general(a, b, (((ca,), (cb,)), ((), ())), preferred_element_type=...]
    psum x1 -> x0, blocking collectives: 11.6 us -> none  [local(): row_squares = lax.psum(partial_squares, 'rep')]
    select_n x0 -> x10, other arithmetic: none -> 5.97 us  [the longest x6 3.54 us: pair(): jnp.where(first, a, b)]
  transfers between devices with their start and end apart: 2 -> 38, of which waited for: 2 -> 11; matrix products, arithmetic and copies ran while one was open for 3% -> 11% of each run, Pallas kernels for 0% -> 15%
where the time goes in v1:
time: 206 us
  starting transfers between devices  77.5 us (38%)
  waiting for transfers between devices  69.1 us (34%)
  Pallas kernels  30.2 us (15%)
  other arithmetic  13.5 us (7%)
  matrix products  8.71 us (4%)
  local copies, waits for them, and re-layouts  5.57 us (3%)
    ppermute x12, waiting for transfers between devices, square(): return lax.ppermute(v, ('rep', 'fs'), pairs)  35.9 us
    ppermute x4, starting transfers between devices, to_far(): return lax.ppermute(v, 'rep', [(0, 2), (3, 1)])  31 us
    pallas_call x3, Pallas kernels, products(): pl.pallas_call(kernel, in_specs=[pl.BlockSpec(memory_space=pltpu.SMEM)] +...  30.2 us
    ppermute x12, starting transfers between devices, square(): return lax.ppermute(v, ('rep', 'fs'), pairs)  20.9 us
    ppermute x3, waiting for transfers between devices, to_mate(): return lax.ppermute(v, 'rep', [(i, i ^ 1) for i in range(4)])  20.3 us
    ppermute x3, starting transfers between devices, to_mate(): return lax.ppermute(v, 'rep', [(i, i ^ 1) for i in range(4)])  15.2 us
    ppermute x4, waiting for transfers between devices, to_far(): return lax.ppermute(v, 'rep', [(0, 2), (3, 1)])  10.9 us
    dot_general x1, matrix products, dot(): lax.dot_general(a, b, (((ca,), (cb,)), ((), ())), preferred_element_type=...  8.71 us
  transfers between devices with their start and end apart: 38, of which 11 were waited for; matrix products, arithmetic and copies ran while one was open for 11% of the time, Pallas kernels for 15%

profile of v1, /device:TPU:0, one launch (start us, length us, event | category | flops | bytes accessed | tf_op | source)
XLA Modules:
  0.0 205.8 jit_solution(15180977282371815209)
XLA Ops:
  0.6 1.4 collective-permute-start.5
  2.1 4.9 %collective-permute-start.1 = (bf16[768,512]{1,0:T(8,128)(2,1)}, bf16[768,512]{1,0:T(8,128)(2,1)S(1)}, u32[]{:S(2)}, u32[]{:S(2)}) collective-permute-start(bf16[768,512]{1,0:T(8,128)(2,1)} %param.6), channel_id=1, source_target_pairs={{0,2},{2,0},{8,10},{10,8},{20,22},{22,20},{28,30},{30,28},{1,3},{3... | collective-permute-start | bytes 2359304 | tf_op jit(solution)/shard_map/ppermute | solution.py:111
  7.0 2.6 %collective-permute-start = (bf16[768,512]{1,0:T(8,128)(2,1)}, bf16[768,512]{1,0:T(8,128)(2,1)}, u32[]{:S(2)}, u32[]{:S(2)}) collective-permute-start(bf16[768,512]{1,0:T(8,128)(2,1)} %param.6), channel_id=1, source_target_pairs={{0,4},{2,6},{8,12},{10,14},{20,16},{22,18},{28,24},{30,26},{1,5},{... | collective-permute-start | bytes 2359304 | tf_op jit(solution)/shard_map/ppermute | solution.py:111
  9.5 1.3 fusion.26.refs_0_
  10.9 1.5 collective-permute-start.32
  12.4 1.8 slice.28
  14.2 1.3 collective-permute-start.11
  15.5 8.3 %collective-permute-done.5 = bf16[768,512]{1,0:T(8,128)(2,1)} collective-permute-done((bf16[768,512]{1,0:T(8,128)(2,1)}, bf16[768,512]{1,0:T(8,128)(2,1)}, u32[]{:S(2)}, u32[]{:S(2)}) %collective-permute-start.5) | collective-permute-done | bytes 786464 | tf_op jit(solution)/shard_map/ppermute | solution.py:111
  23.8 0.9 collective-permute-done.1
  24.7 1.3 collective-permute-start.2
  26.0 1.2 broadcast_select_fusion.6
  27.3 1.9 collective-permute-start.7
  29.2 1.8 fusion.24
  31.6 11.0 %collective-permute-done.2 = bf16[768,512]{1,0:T(8,128)(2,1)S(1)} collective-permute-done((bf16[768,512]{1,0:T(8,128)(2,1)S(1)}, bf16[768,512]{1,0:T(8,128)(2,1)S(1)}, u32[]{:S(2)}, u32[]{:S(2)}) %collective-permute-start.2) | collective-permute-done | bytes 786464 | tf_op jit(solution)/shard_map/ppermute | solution.py:111
  42.7 3.5 %collective-permute-done.7 = bf16[768,512]{1,0:T(8,128)(2,1)S(1)} collective-permute-done((bf16[768,512]{1,0:T(8,128)(2,1)S(1)}, bf16[768,512]{1,0:T(8,128)(2,1)S(1)}, u32[]{:S(2)}, u32[]{:S(2)}) %collective-permute-start.7) | collective-permute-done | bytes 786464 | tf_op jit(solution)/shard_map/ppermute | solution.py:111
  46.9 1.0 slice_select_fusion
  48.8 6.1 %collective-permute-start.33 = (bf16[224,768]{1,0:T(8,128)(2,1)S(1)}, bf16[224,768]{1,0:T(8,128)(2,1)S(1)}, u32[]{:S(2)}, u32[]{:S(2)}) collective-permute-start(bf16[224,768]{1,0:T(8,128)(2,1)S(1)} %fusion.26.refs_0_), channel_id=1, source_target_pairs={{0,16},{24,8},{1,17},{25,9},{2,18},{26,10},{3,19},{27,11},{4,20},{... | collective-permute-start | bytes 1032200 | tf_op jit(solution)/shard_map/ppermute | solution.py:126
  55.1 1.3 collective-permute-start.20
  56.4 1.6 collective-permute-start.13
  58.0 1.1 collective-permute-start.14
  59.2 0.7 copy-done.4
  60.1 10.9 %collective-permute-done.20.refs_15_ = bf16[384,512]{1,0:T(8,128)(2,1)S(1)} collective-permute-done((bf16[384,512]{1,0:T(8,128)(2,1)S(1)}, bf16[384,512]{1,0:T(8,128)(2,1)S(1)}, u32[]{:S(2)}, u32[]{:S(2)}) %collective-permute-start.20) | collective-permute-done | bytes 393248 | tf_op jit(solution)/shard_map/ppermute | solution.py:126
  71.0 1.5 collective-permute-start.21
  72.5 1.4 collective-permute-start.22
  75.3 1.6 broadcast_select_fusion.3
  76.9 6.1 %collective-permute-done.21.refs_16_ = bf16[384,512]{1,0:T(8,128)(2,1)S(1)} collective-permute-done((bf16[384,512]{1,0:T(8,128)(2,1)S(1)}, bf16[384,512]{1,0:T(8,128)(2,1)S(1)}, u32[]{:S(2)}, u32[]{:S(2)}) %collective-permute-start.21) | collective-permute-done | bytes 393248 | tf_op jit(solution)/shard_map/ppermute | solution.py:111
  83.0 1.4 collective-permute-start.23
  84.6 5.1 %collective-permute-done.15.refs_10_ = bf16[384,512]{1,0:T(8,128)(2,1)S(1)} collective-permute-done((bf16[384,512]{1,0:T(8,128)(2,1)S(1)}, bf16[384,512]{1,0:T(8,128)(2,1)S(1)}, u32[]{:S(2)}, u32[]{:S(2)}) %collective-permute-start.15) | collective-permute-done | bytes 393248 | tf_op jit(solution)/shard_map/ppermute | solution.py:111
  90.3 1.5 broadcast_select_fusion.1
  91.9 1.6 collective-permute-start.29
  93.5 1.0 collective-permute-done.23.refs_18_
  94.5 19.9 %collective-permute-start.30 = (bf16[384,768]{1,0:T(8,128)(2,1)}, bf16[384,768]{1,0:T(8,128)(2,1)}, u32[]{:S(2)}, u32[]{:S(2)}) collective-permute-start(bf16[384,768]{1,0:T(8,128)(2,1)} %get-tuple-element.57.refs_0_), channel_id=1, source_target_pairs={{0,16},{24,8},{1,17},{25,9},{2,18},{26,10},{3,19},{27,11},{4,20},{... | collective-permute-start | bytes 1769480 | tf_op jit(solution)/shard_map/ppermute | solution.py:126
  115.2 3.6 %collective-permute-start.10 = (bf16[384,768]{1,0:T(8,128)(2,1)}, bf16[384,768]{1,0:T(8,128)(2,1)}, u32[]{:S(2)}, u32[]{:S(2)}) collective-permute-start(bf16[384,768]{1,0:T(8,128)(2,1)} %get-tuple-element.56.refs_0_), channel_id=1, source_target_pairs={{0,16},{24,8},{1,17},{25,9},{2,18},{26,10},{3,19},{27,11},{4,20},{... | collective-permute-start | bytes 1769480 | tf_op jit(solution)/shard_map/ppermute | solution.py:126
  118.8 0.8 copy-done.26
  119.6 8.7 %fusion.8 = (bf16[768,992]{0,1:T(8,128)(2,1)}, bf16[768,992]{0,1:T(8,128)(2,1)}) fusion(bf16[768,992]{0,1:T(8,128)(2,1)S(1)} %copy-done.8, bf16[768,992]{0,1:T(8,128)(2,1)S(1)} %copy-done.9, bf16[992,4096]{1,0:T(8,128)(2,1)S(1)} %bitcast.11, bf16[768,2048]{1,0:T(8,128)(2,1)S(1)} %get-tuple-element.49, bf16[768,2048]{1,0:T(8,128)(2,1)S(1)} %get-tuple-element.48), kind=kOutput, calls=%fused_computation.17 | convolution fusion | flops 6265135104 | bytes 20512768 | tf_op jit(solution)/shard_map/dot_general | solution.py:14
  128.4 0.8 copy-done.27
  129.1 8.4 %products.5 = (bf16[224,1024]{1,0:T(8,128)(2,1)}, f32[224,1024]{1,0:T(8,128)}) custom-call(s32[3]{0:T(128)} %pad_add_fusion.flags_ref, bf16[224,768]{1,0:T(8,128)(2,1)} %copy-done.10, bf16[224,768]{1,0:T(8,128)(2,1)} %collective-permute-done.32.refs_1_, bf16[224,768]{1,0:T(8,128)(2,1)} %copy-done.28, bf16[768,512]{1,0:T(8,128)(2,1)} %copy-done.1, ...), custom_call_target="tpu_custom_call" | custom-call | flops 2113929216 | bytes 9437184 | tf_op jit(solution)/shard_map/products/pallas_call | solution.py:76
  137.5 11.0 %products.4 = (bf16[384,1024]{1,0:T(8,128)(2,1)}, f32[384,1024]{1,0:T(8,128)}) custom-call(s32[3]{0:T(128)} %pad_add_fusion.flags_ref, bf16[384,768]{1,0:T(8,128)(2,1)} %get-tuple-element.57.refs_0_, bf16[384,768]{1,0:T(8,128)(2,1)} %collective-permute-done.29.refs_1_, bf16[384,768]{1,0:T(8,128)(2,1)} %collective-permute-done.30.refs_2_, ...), custom_call_target="tpu_custom_call" | custom-call | flops 3623878656 | bytes 9437184 | tf_op jit(solution)/shard_map/products/pallas_call | solution.py:76
  148.5 14.6 %collective-permute-start.31 = (bf16[384,1024]{1,0:T(8,128)(2,1)}, bf16[384,1024]{1,0:T(8,128)(2,1)S(1)}, u32[]{:S(2)}, u32[]{:S(2)}) collective-permute-start(bf16[384,1024]{1,0:T(8,128)(2,1)} %get-tuple-element.38), channel_id=1, source_target_pairs={{0,8},{8,0},{16,24},{24,16},{1,9},{9,1},{17,25},{25,17},{2,10},{10... | collective-permute-start | bytes 2359304 | tf_op jit(solution)/shard_map/ppermute | solution.py:129
  163.1 0.8 copy-done.29
  163.9 10.8 %products.3 = (bf16[384,1024]{1,0:T(8,128)(2,1)}, f32[384,1024]{1,0:T(8,128)}) custom-call(s32[3]{0:T(128)} %pad_add_fusion.flags_ref, bf16[384,768]{1,0:T(8,128)(2,1)} %get-tuple-element.56.refs_0_, bf16[384,768]{1,0:T(8,128)(2,1)} %copy-done.29, bf16[384,768]{1,0:T(8,128)(2,1)} %collective-permute-done.10.refs_2_, bf16[768,512]{1,0:T(8,128)(2,1)} %copy-done.1, ...), custom_call_target="tpu_custom_call" | custom-call | flops 3623878656 | bytes 9437184 | tf_op jit(solution)/shard_map/products/pallas_call | solution.py:76
  175.6 6.1 %collective-permute-done.31 = bf16[384,1024]{1,0:T(8,128)(2,1)S(1)} collective-permute-done((bf16[384,1024]{1,0:T(8,128)(2,1)}, bf16[384,1024]{1,0:T(8,128)(2,1)S(1)}, u32[]{:S(2)}, u32[]{:S(2)}) %collective-permute-start.31) | collective-permute-done | bytes 786464 | tf_op jit(solution)/shard_map/ppermute | solution.py:129
  182.0 14.2 %collective-permute-done.28 = bf16[384,1024]{1,0:T(8,128)(2,1)S(1)} collective-permute-done((bf16[384,1024]{1,0:T(8,128)(2,1)}, bf16[384,1024]{1,0:T(8,128)(2,1)S(1)}, u32[]{:S(2)}, u32[]{:S(2)}) %collective-permute-start.28) | collective-permute-done | bytes 786464 | tf_op jit(solution)/shard_map/ppermute | solution.py:129
  196.5 2.0 collective-permute-start.37
  198.5 1.3 collective-permute-start.36
  199.8 1.0 collective-permute-start.35
  200.8 2.5 %pad_maximum_fusion.1 = f32[992,1024]{1,0:T(8,128)} fusion(f32[224,1024]{1,0:T(8,128)S(1)} %get-tuple-element.47, f32[384,1024]{1,0:T(8,128)S(1)} %get-tuple-element.45, f32[384,1024]{1,0:T(8,128)S(1)} %get-tuple-element.43), kind=kLoop, calls=%fused_computation.4 | loop fusion | flops 2031616 | bytes 8126464 | tf_op jit(solution)/shard_map/concatenate | solution.py:213
  203.3 1.9 collective-permute-done.35
  (117 shorter events, 7.5 us)
Async XLA Ops:
  0.6 25.4 %copy-start = (bf16[768,512]{1,0:T(8,128)(2,1)S(1)}, bf16[768,512]{1,0:T(8,128)(2,1)}, u32[]{:S(2)}) copy-start(bf16[768,512]{1,0:T(8,128)(2,1)} %param.6) | copy-start | bytes 2359300
  0.6 23.1 %collective-permute-start.5 = (bf16[768,512]{1,0:T(8,128)(2,1)}, bf16[768,512]{1,0:T(8,128)(2,1)}, u32[]{:S(2)}, u32[]{:S(2)}) collective-permute-start(bf16[768,512]{1,0:T(8,128)(2,1)} %param.6), channel_id=1, source_target_pairs={{4,0},{6,2},{12,8},{14,10},{16,20},{18,22},{24,28},{26,30},{5,1},{... | collective-permute-start | bytes 2359304 | tf_op jit(solution)/shard_map/ppermute | solution.py:111
  2.1 22.6 %collective-permute-start.1 = (bf16[768,512]{1,0:T(8,128)(2,1)}, bf16[768,512]{1,0:T(8,128)(2,1)S(1)}, u32[]{:S(2)}, u32[]{:S(2)}) collective-permute-start(bf16[768,512]{1,0:T(8,128)(2,1)} %param.6), channel_id=1, source_target_pairs={{0,2},{2,0},{8,10},{10,8},{20,22},{22,20},{28,30},{30,28},{1,3},{3... | collective-permute-start | bytes 2359304 | tf_op jit(solution)/shard_map/ppermute | solution.py:111
  7.0 24.6 %collective-permute-start = (bf16[768,512]{1,0:T(8,128)(2,1)}, bf16[768,512]{1,0:T(8,128)(2,1)}, u32[]{:S(2)}, u32[]{:S(2)}) collective-permute-start(bf16[768,512]{1,0:T(8,128)(2,1)} %param.6), channel_id=1, source_target_pairs={{0,4},{2,6},{8,12},{10,14},{20,16},{22,18},{28,24},{30,26},{1,5},{... | collective-permute-start | bytes 2359304 | tf_op jit(solution)/shard_map/ppermute | solution.py:111
  10.8 37.9 %copy-start.10 = (bf16[224,768]{1,0:T(8,128)(2,1)}, bf16[224,768]{1,0:T(8,128)(2,1)S(1)}, u32[]{:S(2)}) copy-start(bf16[224,768]{1,0:T(8,128)(2,1)S(1)} %fusion.26.refs_0_) | copy-start | bytes 1032196
  10.8 18.3 %copy-start.7 = (bf16[768,992]{0,1:T(8,128)(2,1)S(1)}, bf16[768,992]{0,1:T(8,128)(2,1)}, u32[]{:S(2)}) copy-start(bf16[768,992]{0,1:T(8,128)(2,1)} %param.4) | copy-start | bytes 4571140
  10.9 44.2 %collective-permute-start.32 = (bf16[224,768]{1,0:T(8,128)(2,1)S(1)}, bf16[224,768]{1,0:T(8,128)(2,1)}, u32[]{:S(2)}, u32[]{:S(2)}) collective-permute-start(bf16[224,768]{1,0:T(8,128)(2,1)S(1)} %fusion.26.refs_0_), channel_id=1, source_target_pairs={{8,16},{16,8},{9,17},{17,9},{10,18},{18,10},{11,19},{19,11},{12,20... | collective-permute-start | bytes 1032200 | tf_op jit(solution)/shard_map/ppermute | solution.py:123
  14.2 32.7 %collective-permute-start.11 = (bf16[384,512]{1,0:T(8,128)(2,1)}, bf16[384,512]{1,0:T(8,128)(2,1)}, u32[]{:S(2)}, u32[]{:S(2)}) collective-permute-start(bf16[384,512]{1,0:T(8,128)(2,1)} %slice.28), channel_id=1, source_target_pairs={{4,0},{6,2},{12,8},{14,10},{16,20},{18,22},{24,28},{26,30},{5,1},{... | collective-permute-start | bytes 1179656 | tf_op jit(solution)/shard_map/ppermute | solution.py:111
  24.7 17.9 %collective-permute-start.2 = (bf16[768,512]{1,0:T(8,128)(2,1)S(1)}, bf16[768,512]{1,0:T(8,128)(2,1)S(1)}, u32[]{:S(2)}, u32[]{:S(2)}) collective-permute-start(bf16[768,512]{1,0:T(8,128)(2,1)S(1)} %collective-permute-done.1), channel_id=1, source_target_pairs={{0,4},{2,6},{8,12},{10,14},{20,16},{22,18},{28,24},{30,26},{1,5},{... | collective-permute-start | bytes 2359304 | tf_op jit(solution)/shard_map/ppermute | solution.py:111
  27.3 18.9 %collective-permute-start.7 = (bf16[768,512]{1,0:T(8,128)(2,1)S(1)}, bf16[768,512]{1,0:T(8,128)(2,1)S(1)}, u32[]{:S(2)}, u32[]{:S(2)}) collective-permute-start(bf16[768,512]{1,0:T(8,128)(2,1)S(1)} %broadcast_select_fusion.6), channel_id=1, source_target_pairs={{0,2},{2,0},{4,6},{6,4},{8,10},{10,8},{12,14},{14,12},{16,18},{18,... | collective-permute-start | bytes 2359304 | tf_op jit(solution)/shard_map/ppermute | solution.py:111
  31.6 16.4 %collective-permute-start.6 = (bf16[768,512]{1,0:T(8,128)(2,1)S(1)}, bf16[768,512]{1,0:T(8,128)(2,1)S(1)}, u32[]{:S(2)}, u32[]{:S(2)}) collective-permute-start(bf16[768,512]{1,0:T(8,128)(2,1)S(1)} %broadcast_select_fusion.6), channel_id=1, source_target_pairs={{0,1},{1,0},{2,3},{3,2},{4,5},{5,4},{6,7},{7,6},{8,9},{9,8},{10,11... | collective-permute-start | bytes 2359304 | tf_op jit(solution)/shard_map/ppermute | solution.py:120
  42.7 16.4 %copy-start.1 = (bf16[768,512]{1,0:T(8,128)(2,1)}, bf16[768,512]{1,0:T(8,128)(2,1)S(1)}, u32[]{:S(2)}) copy-start(bf16[768,512]{1,0:T(8,128)(2,1)S(1)} %broadcast_select_fusion.8.refs_3_) | copy-start | bytes 2359300
  46.1 2.6 %collective-permute-start.8 = (bf16[768,512]{1,0:T(8,128)(2,1)S(1)}, bf16[768,512]{1,0:T(8,128)(2,1)S(1)}, u32[]{:S(2)}, u32[]{:S(2)}) collective-permute-start(bf16[768,512]{1,0:T(8,128)(2,1)S(1)} %collective-permute-done.7), channel_id=1, source_target_pairs={{0,1},{1,0},{2,3},{3,2},{4,5},{5,4},{6,7},{7,6},{8,9},{9,8},{10,11... | collective-permute-start | bytes 2359304 | tf_op jit(solution)/shard_map/ppermute | solution.py:120
  46.2 11.7 %collective-permute-start.3 = (bf16[768,512]{1,0:T(8,128)(2,1)S(1)}, bf16[768,512]{1,0:T(8,128)(2,1)S(1)}, u32[]{:S(2)}, u32[]{:S(2)}) collective-permute-start(bf16[768,512]{1,0:T(8,128)(2,1)S(1)} %broadcast_select_fusion.8.refs_3_), channel_id=1, source_target_pairs={{0,1},{1,0},{2,3},{3,2},{4,5},{5,4},{6,7},{7,6},{8,9},{9,8},{10,11... | collective-permute-start | bytes 2359304 | tf_op jit(solution)/shard_map/ppermute | solution.py:120
  46.8 12.2 %collective-permute-start.4 = (bf16[768,512]{1,0:T(8,128)(2,1)S(1)}, bf16[768,512]{1,0:T(8,128)(2,1)S(1)}, u32[]{:S(2)}, u32[]{:S(2)}) collective-permute-start(bf16[768,512]{1,0:T(8,128)(2,1)S(1)} %broadcast_select_fusion.7.refs_4_), channel_id=1, source_target_pairs={{0,1},{1,0},{2,3},{3,2},{4,5},{5,4},{6,7},{7,6},{8,9},{9,8},{10,11... | collective-permute-start | bytes 2359304 | tf_op jit(solution)/shard_map/ppermute | solution.py:120
  48.0 8.4 %collective-permute-start.12 = (bf16[384,512]{1,0:T(8,128)(2,1)S(1)}, bf16[384,512]{1,0:T(8,128)(2,1)S(1)}, u32[]{:S(2)}, u32[]{:S(2)}) collective-permute-start(bf16[384,512]{1,0:T(8,128)(2,1)S(1)} %slice_select_fusion), channel_id=1, source_target_pairs={{8,16},{16,8},{9,17},{17,9},{10,18},{18,10},{11,19},{19,11},{12,20... | collective-permute-start | bytes 1179656 | tf_op jit(solution)/shard_map/ppermute | solution.py:123
  48.8 23.7 %collective-permute-start.33 = (bf16[224,768]{1,0:T(8,128)(2,1)S(1)}, bf16[224,768]{1,0:T(8,128)(2,1)S(1)}, u32[]{:S(2)}, u32[]{:S(2)}) collective-permute-start(bf16[224,768]{1,0:T(8,128)(2,1)S(1)} %fusion.26.refs_0_), channel_id=1, source_target_pairs={{0,16},{24,8},{1,17},{25,9},{2,18},{26,10},{3,19},{27,11},{4,20},{... | collective-permute-start | bytes 1032200 | tf_op jit(solution)/shard_map/ppermute | solution.py:126
  55.1 15.9 %collective-permute-start.20 = (bf16[384,512]{1,0:T(8,128)(2,1)S(1)}, bf16[384,512]{1,0:T(8,128)(2,1)S(1)}, u32[]{:S(2)}, u32[]{:S(2)}) collective-permute-start(bf16[384,512]{1,0:T(8,128)(2,1)S(1)} %slice_select_fusion), channel_id=1, source_target_pairs={{0,16},{24,8},{1,17},{25,9},{2,18},{26,10},{3,19},{27,11},{4,20},{... | collective-permute-start | bytes 1179656 | tf_op jit(solution)/shard_map/ppermute | solution.py:126
  56.4 17.5 %collective-permute-start.13 = (bf16[384,512]{1,0:T(8,128)(2,1)S(1)}, bf16[384,512]{1,0:T(8,128)(2,1)S(1)}, u32[]{:S(2)}, u32[]{:S(2)}) collective-permute-start(bf16[384,512]{1,0:T(8,128)(2,1)S(1)} %collective-permute-done.12.refs_7_), channel_id=1, source_target_pairs={{0,2},{2,0},{4,6},{6,4},{8,10},{10,8},{12,14},{14,12},{16,18},{18,... | collective-permute-start | bytes 1179656 | tf_op jit(solution)/shard_map/ppermute | solution.py:111
  58.0 15.9 %collective-permute-start.14 = (bf16[384,512]{1,0:T(8,128)(2,1)S(1)}, bf16[384,512]{1,0:T(8,128)(2,1)S(1)}, u32[]{:S(2)}, u32[]{:S(2)}) collective-permute-start(bf16[384,512]{1,0:T(8,128)(2,1)S(1)} %collective-permute-done.12.refs_7_), channel_id=1, source_target_pairs={{0,4},{2,6},{4,0},{6,2},{8,12},{10,14},{12,8},{14,10},{16,20},{18,... | collective-permute-start | bytes 1179656 | tf_op jit(solution)/shard_map/ppermute | solution.py:111
  59.1 15.4 %collective-permute-start.16 = (bf16[384,512]{1,0:T(8,128)(2,1)S(1)}, bf16[384,512]{1,0:T(8,128)(2,1)S(1)}, u32[]{:S(2)}, u32[]{:S(2)}) collective-permute-start(bf16[384,512]{1,0:T(8,128)(2,1)S(1)} %collective-permute-done.12.refs_7_), channel_id=1, source_target_pairs={{0,1},{1,0},{2,3},{3,2},{4,5},{5,4},{6,7},{7,6},{8,9},{9,8},{10,11... | collective-permute-start | bytes 1179656 | tf_op jit(solution)/shard_map/ppermute | solution.py:120
  71.0 12.0 %collective-permute-start.21 = (bf16[384,512]{1,0:T(8,128)(2,1)S(1)}, bf16[384,512]{1,0:T(8,128)(2,1)S(1)}, u32[]{:S(2)}, u32[]{:S(2)}) collective-permute-start(bf16[384,512]{1,0:T(8,128)(2,1)S(1)} %collective-permute-done.20.refs_15_), channel_id=1, source_target_pairs={{0,2},{2,0},{4,6},{6,4},{8,10},{10,8},{12,14},{14,12},{16,18},{18,... | collective-permute-start | bytes 1179656 | tf_op jit(solution)/shard_map/ppermute | solution.py:111
  72.5 10.5 %collective-permute-start.22 = (bf16[384,512]{1,0:T(8,128)(2,1)S(1)}, bf16[384,512]{1,0:T(8,128)(2,1)S(1)}, u32[]{:S(2)}, u32[]{:S(2)}) collective-permute-start(bf16[384,512]{1,0:T(8,128)(2,1)S(1)} %collective-permute-done.20.refs_15_), channel_id=1, source_target_pairs={{0,4},{2,6},{4,0},{6,2},{8,12},{10,14},{12,8},{14,10},{16,20},{18,... | collective-permute-start | bytes 1179656 | tf_op jit(solution)/shard_map/ppermute | solution.py:111
  73.9 10.6 %collective-permute-start.24 = (bf16[384,512]{1,0:T(8,128)(2,1)S(1)}, bf16[384,512]{1,0:T(8,128)(2,1)S(1)}, u32[]{:S(2)}, u32[]{:S(2)}) collective-permute-start(bf16[384,512]{1,0:T(8,128)(2,1)S(1)} %collective-permute-done.20.refs_15_), channel_id=1, source_target_pairs={{0,1},{1,0},{2,3},{3,2},{4,5},{5,4},{6,7},{7,6},{8,9},{9,8},{10,11... | collective-permute-start | bytes 1179656 | tf_op jit(solution)/shard_map/ppermute | solution.py:120
  73.9 15.8 %collective-permute-start.15 = (bf16[384,512]{1,0:T(8,128)(2,1)S(1)}, bf16[384,512]{1,0:T(8,128)(2,1)S(1)}, u32[]{:S(2)}, u32[]{:S(2)}) collective-permute-start(bf16[384,512]{1,0:T(8,128)(2,1)S(1)} %collective-permute-done.14.refs_9_), channel_id=1, source_target_pairs={{0,2},{2,0},{4,6},{6,4},{8,10},{10,8},{12,14},{14,12},{16,18},{18,... | collective-permute-start | bytes 1179656 | tf_op jit(solution)/shard_map/ppermute | solution.py:111
  74.5 15.2 %collective-permute-start.17 = (bf16[384,512]{1,0:T(8,128)(2,1)S(1)}, bf16[384,512]{1,0:T(8,128)(2,1)S(1)}, u32[]{:S(2)}, u32[]{:S(2)}) collective-permute-start(bf16[384,512]{1,0:T(8,128)(2,1)S(1)} %collective-permute-done.13.refs_8_), channel_id=1, source_target_pairs={{0,1},{1,0},{2,3},{3,2},{4,5},{5,4},{6,7},{7,6},{8,9},{9,8},{10,11... | collective-permute-start | bytes 1179656 | tf_op jit(solution)/shard_map/ppermute | solution.py:120
  75.3 44.3 %slice-start = ((s8[8126464]{0:T(1024)(128)(4,1)}), s8[3932160]{0:T(1024)(128)(4,1)S(1)}, s32[]{:S(2)}) async-start(s8[8126464]{0:T(1024)(128)(4,1)} %bitcast.10), calls=%async_computation | async-start | bytes 7864320
  83.0 8.9 %collective-permute-start.18 = (bf16[384,512]{1,0:T(8,128)(2,1)S(1)}, bf16[384,512]{1,0:T(8,128)(2,1)S(1)}, u32[]{:S(2)}, u32[]{:S(2)}) collective-permute-start(bf16[384,512]{1,0:T(8,128)(2,1)S(1)} %collective-permute-done.14.refs_9_), channel_id=1, source_target_pairs={{0,1},{1,0},{2,3},{3,2},{4,5},{5,4},{6,7},{7,6},{8,9},{9,8},{10,11... | collective-permute-start | bytes 1179656 | tf_op jit(solution)/shard_map/ppermute | solution.py:120
  83.0 11.5 %collective-permute-start.23 = (bf16[384,512]{1,0:T(8,128)(2,1)S(1)}, bf16[384,512]{1,0:T(8,128)(2,1)S(1)}, u32[]{:S(2)}, u32[]{:S(2)}) collective-permute-start(bf16[384,512]{1,0:T(8,128)(2,1)S(1)} %collective-permute-done.21.refs_16_), channel_id=1, source_target_pairs={{0,4},{2,6},{4,0},{6,2},{8,12},{10,14},{12,8},{14,10},{16,20},{18,... | collective-permute-start | bytes 1179656 | tf_op jit(solution)/shard_map/ppermute | solution.py:111
  84.5 30.0 %collective-permute-start.25 = (bf16[384,512]{1,0:T(8,128)(2,1)S(1)}, bf16[384,512]{1,0:T(8,128)(2,1)S(1)}, u32[]{:S(2)}, u32[]{:S(2)}) collective-permute-start(bf16[384,512]{1,0:T(8,128)(2,1)S(1)} %collective-permute-done.21.refs_16_), channel_id=1, source_target_pairs={{0,1},{1,0},{2,3},{3,2},{4,5},{5,4},{6,7},{7,6},{8,9},{9,8},{10,11... | collective-permute-start | bytes 1179656 | tf_op jit(solution)/shard_map/ppermute | solution.py:120
  89.8 25.4 %collective-permute-start.26 = (bf16[384,512]{1,0:T(8,128)(2,1)S(1)}, bf16[384,512]{1,0:T(8,128)(2,1)S(1)}, u32[]{:S(2)}, u32[]{:S(2)}) collective-permute-start(bf16[384,512]{1,0:T(8,128)(2,1)S(1)} %collective-permute-done.22.refs_17_), channel_id=1, source_target_pairs={{0,1},{1,0},{2,3},{3,2},{4,5},{5,4},{6,7},{7,6},{8,9},{9,8},{10,11... | collective-permute-start | bytes 1179656 | tf_op jit(solution)/shard_map/ppermute | solution.py:120
  89.8 29.1 %collective-permute-start.19 = (bf16[384,512]{1,0:T(8,128)(2,1)S(1)}, bf16[384,512]{1,0:T(8,128)(2,1)S(1)}, u32[]{:S(2)}, u32[]{:S(2)}) collective-permute-start(bf16[384,512]{1,0:T(8,128)(2,1)S(1)} %collective-permute-done.15.refs_10_), channel_id=1, source_target_pairs={{0,1},{1,0},{2,3},{3,2},{4,5},{5,4},{6,7},{7,6},{8,9},{9,8},{10,11... | collective-permute-start | bytes 1179656 | tf_op jit(solution)/shard_map/ppermute | solution.py:120
  90.3 29.3 %slice-start.1 = ((s8[8126464]{0:T(1024)(128)(4,1)}), s8[4194304]{0:T(1024)(128)(4,1)S(1)}, s32[]{:S(2)}) async-start(s8[8126464]{0:T(1024)(128)(4,1)} %bitcast.10), calls=%async_computation.1 | async-start | bytes 8388608
  90.3 29.3 %copy-start.8 = (bf16[768,992]{0,1:T(8,128)(2,1)S(1)}, bf16[768,992]{0,1:T(8,128)(2,1)}, u32[]{:S(2)}) copy-start(bf16[768,992]{0,1:T(8,128)(2,1)} %param.4) | copy-start | bytes 4571140
  91.9 36.4 %copy-start.22 = (bf16[384,512]{1,0:T(8,128)(2,1)}, bf16[384,512]{1,0:T(8,128)(2,1)S(1)}, u32[]{:S(2)}) copy-start(bf16[384,512]{1,0:T(8,128)(2,1)S(1)} %collective-permute-done.18.refs_13_) | copy-start | bytes 1179652
  91.9 45.6 %collective-permute-start.29 = (bf16[384,768]{1,0:T(8,128)(2,1)}, bf16[384,768]{1,0:T(8,128)(2,1)}, u32[]{:S(2)}, u32[]{:S(2)}) collective-permute-start(bf16[384,768]{1,0:T(8,128)(2,1)} %get-tuple-element.57.refs_0_), channel_id=1, source_target_pairs={{8,16},{16,8},{9,17},{17,9},{10,18},{18,10},{11,19},{19,11},{12,20... | collective-permute-start | bytes 1769480 | tf_op jit(solution)/shard_map/ppermute | solution.py:123
  94.5 33.8 %copy-start.23 = (bf16[384,512]{1,0:T(8,128)(2,1)}, bf16[384,512]{1,0:T(8,128)(2,1)S(1)}, u32[]{:S(2)}) copy-start(bf16[384,512]{1,0:T(8,128)(2,1)S(1)} %collective-permute-done.23.refs_18_) | copy-start | bytes 1179652
  94.5 42.9 %collective-permute-start.30 = (bf16[384,768]{1,0:T(8,128)(2,1)}, bf16[384,768]{1,0:T(8,128)(2,1)}, u32[]{:S(2)}, u32[]{:S(2)}) collective-permute-start(bf16[384,768]{1,0:T(8,128)(2,1)} %get-tuple-element.57.refs_0_), channel_id=1, source_target_pairs={{0,16},{24,8},{1,17},{25,9},{2,18},{26,10},{3,19},{27,11},{4,20},{... | collective-permute-start | bytes 1769480 | tf_op jit(solution)/shard_map/ppermute | solution.py:126
  114.5 48.6 %collective-permute-start.9 = (bf16[384,768]{1,0:T(8,128)(2,1)}, bf16[384,768]{1,0:T(8,128)(2,1)S(1)}, u32[]{:S(2)}, u32[]{:S(2)}) collective-permute-start(bf16[384,768]{1,0:T(8,128)(2,1)} %get-tuple-element.56.refs_0_), channel_id=1, source_target_pairs={{8,16},{16,8},{9,17},{17,9},{10,18},{18,10},{11,19},{19,11},{12,20... | collective-permute-start | bytes 1769480 | tf_op jit(solution)/shard_map/ppermute | solution.py:123
  115.2 47.9 %collective-permute-start.10 = (bf16[384,768]{1,0:T(8,128)(2,1)}, bf16[384,768]{1,0:T(8,128)(2,1)}, u32[]{:S(2)}, u32[]{:S(2)}) collective-permute-start(bf16[384,768]{1,0:T(8,128)(2,1)} %get-tuple-element.56.refs_0_), channel_id=1, source_target_pairs={{0,16},{24,8},{1,17},{25,9},{2,18},{26,10},{3,19},{27,11},{4,20},{... | collective-permute-start | bytes 1769480 | tf_op jit(solution)/shard_map/ppermute | solution.py:126
  118.8 9.5 %collective-permute-start.27 = (bf16[384,512]{1,0:T(8,128)(2,1)S(1)}, bf16[384,512]{1,0:T(8,128)(2,1)S(1)}, u32[]{:S(2)}, u32[]{:S(2)}) collective-permute-start(bf16[384,512]{1,0:T(8,128)(2,1)S(1)} %collective-permute-done.23.refs_18_), channel_id=1, source_target_pairs={{0,1},{1,0},{2,3},{3,2},{4,5},{5,4},{6,7},{7,6},{8,9},{9,8},{10,11... | collective-permute-start | bytes 1179656 | tf_op jit(solution)/shard_map/ppermute | solution.py:120
  137.5 38.0 %collective-permute-start.34 = (bf16[224,1024]{1,0:T(8,128)(2,1)}, bf16[224,1024]{1,0:T(8,128)(2,1)S(1)}, u32[]{:S(2)}, u32[]{:S(2)}) collective-permute-start(bf16[224,1024]{1,0:T(8,128)(2,1)} %get-tuple-element.41), channel_id=1, source_target_pairs={{0,8},{8,0},{16,24},{24,16},{1,9},{9,1},{17,25},{25,17},{2,10},{10... | collective-permute-start | bytes 1376264 | tf_op jit(solution)/shard_map/ppermute | solution.py:129
  148.5 26.9 %copy-start.11 = (f32[224,1024]{1,0:T(8,128)S(1)}, f32[224,1024]{1,0:T(8,128)}, u32[]{:S(2)}) copy-start(f32[224,1024]{1,0:T(8,128)} %get-tuple-element.40) | copy-start | bytes 2752516
  148.5 33.2 %collective-permute-start.31 = (bf16[384,1024]{1,0:T(8,128)(2,1)}, bf16[384,1024]{1,0:T(8,128)(2,1)S(1)}, u32[]{:S(2)}, u32[]{:S(2)}) collective-permute-start(bf16[384,1024]{1,0:T(8,128)(2,1)} %get-tuple-element.38), channel_id=1, source_target_pairs={{0,8},{8,0},{16,24},{24,16},{1,9},{9,1},{17,25},{25,17},{2,10},{10... | collective-permute-start | bytes 2359304 | tf_op jit(solution)/shard_map/ppermute | solution.py:129
  174.8 21.4 %collective-permute-start.28 = (bf16[384,1024]{1,0:T(8,128)(2,1)}, bf16[384,1024]{1,0:T(8,128)(2,1)S(1)}, u32[]{:S(2)}, u32[]{:S(2)}) collective-permute-start(bf16[384,1024]{1,0:T(8,128)(2,1)} %get-tuple-element.36), channel_id=1, source_target_pairs={{0,8},{8,0},{16,24},{24,16},{1,9},{9,1},{17,25},{25,17},{2,10},{10... | collective-permute-start | bytes 2359304 | tf_op jit(solution)/shard_map/ppermute | solution.py:129
  196.5 6.7 %collective-permute-start.37 = (f32[992]{0:T(1024)S(1)}, f32[992]{0:T(1024)S(1)}, u32[]{:S(2)}, u32[]{:S(2)}) collective-permute-start(f32[992]{0:T(1024)S(1)} %pad_maximum_fusion.8), channel_id=1, source_target_pairs={{0,24},{8,0},{16,8},{24,16},{1,25},{9,1},{17,9},{25,17},{2,26},{10... | collective-permute-start | bytes 11912 | tf_op jit(solution)/shard_map/ppermute | solution.py:210
  198.5 4.8 %collective-permute-start.36 = (f32[992]{0:T(1024)S(1)}, f32[992]{0:T(1024)S(1)}, u32[]{:S(2)}, u32[]{:S(2)}) collective-permute-start(f32[992]{0:T(1024)S(1)} %pad_maximum_fusion.8), channel_id=1, source_target_pairs={{0,16},{8,24},{16,0},{24,8},{1,17},{9,25},{17,1},{25,9},{2,18},{10... | collective-permute-start | bytes 11912 | tf_op jit(solution)/shard_map/ppermute | solution.py:210
  199.8 5.4 %collective-permute-start.35 = (f32[992]{0:T(1024)S(1)}, f32[992]{0:T(1024)S(1)}, u32[]{:S(2)}, u32[]{:S(2)}) collective-permute-start(f32[992]{0:T(1024)S(1)} %pad_maximum_fusion.8), channel_id=1, source_target_pairs={{0,8},{8,16},{16,24},{24,0},{1,9},{9,17},{17,25},{25,1},{2,10},{10... | collective-permute-start | bytes 11912 | tf_op jit(solution)/shard_map/ppermute | solution.py:210
  (22 other events, 123.0 us)
